TPU v7x, 32 devices: a whole 2x2x4 slice. The times are simulated.
32 devices in a mesh: rep: 2 (over x), fs: 8 (over z, y), tp: 2 (over core).
Axes of the slice: x: 2, y: 2, z: 4, core: 2. Of those that a mesh axis runs over, the one named last changes fastest.
Arguments:
- inputs: bfloat16 [4096, 2048], P(('rep', 'fs', 'tp')), may hold values from -6 to 6
- cotangent: bfloat16 [4096, 2048], P(('rep', 'fs', 'tp')), may hold values from -6 to 6
- up_weight: bfloat16 [2048, 4096], P('fs', 'tp'), may hold values from -0.125 to 0.125
- down_weight: bfloat16 [4096, 2048], P('tp', 'fs'), may hold values from -0.09375 to 0.09375
Outputs:
- input_grad: bfloat16 [4096, 2048], P(('rep', 'fs', 'tp'))
- up_grad: float32 [2048, 4096], P('fs', 'tp')
- down_grad: float32 [4096, 2048], P('tp', 'fs')
All inputs are finite; a program needn't handle non-finite values.
Results may differ from a plain program's by a relative error of at most 0.013.
Values may be sent and summed in bfloat16 or wider, within the bound.
A program may use at most 128 MiB of HBM per device.

v0:
```python
import math
import jax
import jax.numpy as jnp
from jax import lax
from jax.sharding import PartitionSpec as P


def shards(inputs, cotangent, up_weight, down_weight):
    input_rows, grad_rows = (
        lax.all_gather(inputs, "tp", axis=0, tiled=True),
        lax.all_gather(cotangent, "tp", axis=0, tiled=True),
    )
    up_whole = lax.all_gather(up_weight, "fs", axis=0, tiled=True)
    pre_active = jnp.dot(input_rows, up_whole, preferred_element_type=jnp.float32)
    active = jnp.maximum(pre_active, 0.0)
    activation = (active * active).astype(jnp.bfloat16)
    columns = grad_rows
    activation_grad = lax.dot_general(
        columns,
        lax.all_gather(down_weight, "fs", axis=1, tiled=True),
        (((1,), (1,)), ((), ())),
        preferred_element_type=jnp.float32,
    )
    pre_grad = (2.0 * active * activation_grad).astype(jnp.bfloat16)
    partial_sum = lax.dot_general(
        pre_grad, up_whole, (((1,), (1,)), ((), ())), preferred_element_type=jnp.float32
    )
    input_grad = lax.psum_scatter(
        lax.optimization_barrier(partial_sum.astype(jnp.bfloat16))
        .astype(jnp.float32)
        .astype(jnp.bfloat16),
        "tp",
        scatter_dimension=0,
        tiled=True,
    )
    rep_count = lax.axis_size("rep")
    fs_count = lax.axis_size("fs")
    total_tokens = inputs.shape[0] * rep_count * fs_count * lax.axis_size("tp")
    loss_scale = 1.0 / math.sqrt(total_tokens)
    down_partial = lax.dot_general(
        activation, grad_rows, (((0,), (0,)), ((), ())), preferred_element_type=jnp.float32
    )
    columns = input_rows
    up_piece = lax.psum_scatter(
        lax.dot_general(
            columns, pre_grad, (((0,), (0,)), ((), ())), preferred_element_type=jnp.float32
        ),
        "fs",
        scatter_dimension=0,
        tiled=True,
    )
    down_piece = lax.psum_scatter(down_partial, "fs", scatter_dimension=1, tiled=True)
    up_grad, down_grad = lax.psum((up_piece, down_piece), "rep")
    return (input_grad, up_grad * loss_scale, down_grad * loss_scale)


def solution(mesh):
    placed = (
        P(("rep", "fs", "tp"), None),
        P(("rep", "fs", "tp"), None),
        P("fs", "tp"),
        P("tp", "fs"),
    )
    return jax.shard_map(
        shards,
        mesh=mesh,
        in_specs=placed,
        out_specs=(P(("rep", "fs", "tp"), None), P("fs", "tp"), P("tp", "fs")),
        check_vma=False,
    )
```

profile of v0, /device:TPU:0, one launch (start us, length us, event | category | flops | bytes accessed | tf_op | source)
XLA Modules:
  0.0 978.7 jit_solution(5026646738183738570)
XLA Ops:
  7.2 0.7 all-gather.5.cloned.1.call-update
  7.9 0.7 all-gather.7.cloned.1.call-update
  8.7 0.7 all-gather.9.cloned.1.call-update
  9.4 0.5 all-gather.11.cloned.1.call-update
  10.0 11.3 %all-gather.5.cloned.1.call-done = bf16[256,2048]{1,0:T(8,128)(2,1)} async-done(((bf16[128,2048]{1,0:T(8,128)(2,1)}), bf16[256,2048]{1,0:T(8,128)(2,1)}) %all-gather.5.cloned.1.call-update) | async-done | bytes 1048592 | tf_op jit(solution)/shard_map/all_gather | solution.py:10
  21.3 127.8 %all-gather.7.cloned.1.call-done = bf16[2048,2048]{1,0:T(8,128)(2,1)} async-done(((bf16[256,2048]{1,0:T(8,128)(2,1)}), bf16[2048,2048]{1,0:T(8,128)(2,1)}) %all-gather.7.cloned.1.call-update) | async-done | bytes 8388624 | tf_op jit(solution)/shard_map/all_gather | solution.py:13
  149.1 6.1 convolution_maximum_fusion
  155.2 2.7 all-gather.9.cloned.1.call-done
  157.9 9.4 fusion.1
  167.3 0.0 reduce-scatter.6.cloned.1.call-start
  167.3 118.6 %all-gather.11.cloned.1.call-done = bf16[2048,2048]{1,0:T(8,128)(2,1)} async-done(((bf16[2048,256]{1,0:T(8,128)(2,1)}), bf16[2048,2048]{1,0:T(8,128)(2,1)}) %all-gather.11.cloned.1.call-update) | async-done | bytes 8388624 | tf_op jit(solution)/shard_map/all_gather | solution.py:20
  285.9 6.1 fusion
  292.0 1.0 copy-done.1
  293.0 8.1 convolution_bitcast_fusion
  301.1 0.0 all-reduce.3.cloned.1.call-start
  301.2 266.8 %reduce-scatter.8.cloned.1.call-done = f32[2048,256]{1,0:T(8,128)} async-done(((f32[2048,2048]{1,0:T(8,128)}), f32[2048,256]{1,0:T(8,128)}) %reduce-scatter.8.cloned.1.call-update) | async-done | bytes 2097168 | tf_op jit(solution)/shard_map/reduce_scatter | solution.py:52
  568.0 283.1 %reduce-scatter.6.cloned.1.call-done = f32[256,2048]{0,1:T(8,128)} async-done(((f32[2048,2048]{0,1:T(8,128)}), f32[256,2048]{0,1:T(8,128)}) %reduce-scatter.6.cloned.1.call-update) | async-done | bytes 2097168 | tf_op jit(solution)/shard_map/reduce_scatter | solution.py:44
  851.2 1.2 copy-done.2
  852.3 6.7 convolution_convert_fusion
  859.1 101.6 %all-reduce.3.cloned.1.call-done = (f32[256,2048]{0,1:T(8,128)}, f32[2048,256]{1,0:T(8,128)}) async-done(((f32[256,2048]{0,1:T(8,128)}, f32[2048,256]{1,0:T(8,128)}), (f32[256,2048]{0,1:T(8,128)}, f32[2048,256]{1,0:T(8,128)})) %all-reduce.3.cloned.1.call-update) | async-done | bytes 4194320 | tf_op jit(solution)/shard_map/psum | solution.py:53
  960.6 1.7 broadcast_multiply_fusion.1
  962.4 1.8 copy.7
  964.2 3.0 broadcast_multiply_fusion
  967.2 4.7 reduce-scatter.4.cloned.1.call-done
  (14 shorter events, 0.3 us)
Async XLA Ops:
  7.2 14.1 %all-gather.5.cloned.1.call-start = ((), (), s32[]{:S(2)}) async-start(), calls=%async_computation.3 | async-start | bytes 1572864 | tf_op jit(solution)/shard_map/all_gather | solution.py:10
  7.9 141.2 %all-gather.7.cloned.1.call-start = ((), (), s32[]{:S(2)}) async-start(), calls=%async_computation.4 | async-start | bytes 9437184 | tf_op jit(solution)/shard_map/all_gather | solution.py:13
  8.6 149.3 %all-gather.9.cloned.1.call-start = ((), (), s32[]{:S(2)}) async-start(), calls=%async_computation.5 | async-start | bytes 1572864 | tf_op jit(solution)/shard_map/all_gather | solution.py:11
  9.4 276.6 %all-gather.11.cloned.1.call-start = ((), (), s32[]{:S(2)}) async-start(), calls=%async_computation.6 | async-start | bytes 9437184 | tf_op jit(solution)/shard_map/all_gather | solution.py:20
  10.0 558.1 %reduce-scatter.8.cloned.1.call-start = ((), (), s32[]{:S(2)}) async-start(), calls=%async_computation.9 | async-start | bytes 18874368 | tf_op jit(solution)/shard_map/reduce_scatter | solution.py:52
  167.3 125.7 %copy-start = (bf16[256,2048]{1,0:T(8,128)(2,1)S(1)}, bf16[256,2048]{1,0:T(8,128)(2,1)}, u32[]{:S(2)}) copy-start(bf16[256,2048]{1,0:T(8,128)(2,1)} %all-gather.5.cloned.1.call-done) | copy-start | bytes 3145732
  167.3 683.8 %reduce-scatter.6.cloned.1.call-start = ((), (), s32[]{:S(2)}) async-start(), calls=%async_computation.8 | async-start | bytes 18874368 | tf_op jit(solution)/shard_map/reduce_scatter | solution.py:44
  292.0 1.0 copy-start.1
  301.1 659.5 %all-reduce.3.cloned.1.call-start = ((), (), s32[]{:S(2)}) async-start(), calls=%async_computation.10 | async-start | bytes 8388608 | tf_op jit(solution)/shard_map/psum | solution.py:53
  851.1 1.2 copy-start.2
  851.1 120.8 %reduce-scatter.4.cloned.1.call-start = ((), (), s32[]{:S(2)}) async-start(), calls=%async_computation.7 | async-start | bytes 1572864 | tf_op jit(solution)/shard_map/reduce_scatter | solution.py:28
Sparse Core Ops, SparseCore 0:
  9.5 11.7 all-gather.4
  23.4 125.6 all-gather.6
  150.7 7.1 all-gather.8
  159.8 126.0 all-gather.10
  289.6 278.3 reduce-scatter.7
  571.7 279.3 reduce-scatter.5
  853.6 107.0 all-reduce.2
  963.4 8.3 reduce-scatter.3
where the time goes:
time: 979 us
  waiting for transfers between devices  919 us (94%)
  matrix products  36.3 us (4%)
  between operations  14.2 us (1%)
    reduce_scatter x1, waiting for transfers between devices, shards(): lax.psum_scatter(lax.dot_general(columns, pre_grad, (((0,), (0,)), ((), (...  283 us
    reduce_scatter x1, waiting for transfers between devices, shards(): lax.psum_scatter(down_partial, 'fs', scatter_dimension=1, tiled=True)  267 us
    all_gather x1, waiting for transfers between devices, shards(): up_whole = lax.all_gather(up_weight, 'fs', axis=0, tiled=True)  128 us
    all_gather x1, waiting for transfers between devices, shards(): lax.all_gather(down_weight, 'fs', axis=1, tiled=True)  119 us
    psum x1, waiting for transfers between devices, shards(): up_grad, down_grad = lax.psum((up_piece, down_piece), 'rep')  102 us
  transfers between devices with their start and end apart: 8, of which 8 were waited for; matrix products, arithmetic and copies ran while one was open for 4% of the time, Pallas kernels for 0%

commit v1 on v0

--- a/solution.py
+++ b/solution.py
@@ -10,7 +10,12 @@
         lax.all_gather(inputs, "tp", axis=0, tiled=True),
         lax.all_gather(cotangent, "tp", axis=0, tiled=True),
     )
-    up_whole = lax.all_gather(up_weight, "fs", axis=0, tiled=True)
+    ring = [up_weight]
+    for hop in range(7):
+        ring.append(lax.ppermute(ring[-1], "fs", [(dev, (dev + 1) % 8) for dev in range(8)]))
+    up_whole = jnp.roll(
+        jnp.concatenate(ring[::-1], axis=0), (lax.axis_index("fs") + 1) * ring[0].shape[0], axis=0
+    )
     pre_active = jnp.dot(input_rows, up_whole, preferred_element_type=jnp.float32)
     active = jnp.maximum(pre_active, 0.0)
     activation = (active * active).astype(jnp.bfloat16)

time: 979 us -> 1020 us (1.042)
  local copies, waits for them, and re-layouts: 3.94 us -> 31.5 us
    ppermute x0 -> x7, waiting for transfers between devices: none -> 271 us  [shards(): lax.ppermute(ring[-1], 'fs', [(dev, (dev + 1) % 8) for dev in range(8)])]
    all_gather x1 -> x0, waiting for transfers between devices: 128 us -> none  [shards(): up_whole = lax.all_gather(up_weight, 'fs', axis=0, tiled=True)]
    all_gather x1, waiting for transfers between devices: 119 us -> 0.02 us  [shards(): lax.all_gather(down_weight, 'fs', axis=1, tiled=True)]
    unnamed x7 -> x36, local copies, waits for them, and re-layouts: 3.94 us -> 30.4 us
    all_gather x1, waiting for transfers between devices: 11.3 us -> 0.01 us  [shards(): lax.all_gather(inputs, 'tp', axis=0, tiled=True)]
  transfers between devices with their start and end apart: 8 -> 14, of which waited for: 8 -> 11; matrix products, arithmetic and copies ran while one was open for 4% -> 7% of each run, Pallas kernels for 0% -> 0%
where the time goes in v1:
time: 1020 us
  waiting for transfers between devices  928 us (91%)
  matrix products  36.5 us (4%)
  local copies, waits for them, and re-layouts  31.5 us (3%)
  between operations  14.2 us (1%)
    reduce_scatter x1, waiting for transfers between devices, shards(): lax.psum_scatter(lax.dot_general(columns, pre_grad, (((0,), (0,)), ((), (...  283 us
    ppermute x7, waiting for transfers between devices, shards(): lax.ppermute(ring[-1], 'fs', [(dev, (dev + 1) % 8) for dev in range(8)])  271 us
    reduce_scatter x1, waiting for transfers between devices, shards(): lax.psum_scatter(down_partial, 'fs', scatter_dimension=1, tiled=True)  265 us
    psum x1, waiting for transfers between devices, shards(): up_grad, down_grad = lax.psum((up_piece, down_piece), 'rep')  103 us
    unnamed x36, local copies, waits for them, and re-layouts  30.4 us
  transfers between devices with their start and end apart: 14, of which 11 were waited for; matrix products, arithmetic and copies ran while one was open for 7% of the time, Pallas kernels for 0%

profile of v1, /device:TPU:0, one launch (start us, length us, event | category | flops | bytes accessed | tf_op | source)
XLA Modules:
  0.0 1018.1 jit_solution(11654341383384322227)
XLA Ops:
  9.4 3.0 collective-permute-start
  12.5 26.4 %collective-permute-done = bf16[256,2048]{1,0:T(8,128)(2,1)S(1)} collective-permute-done((bf16[256,2048]{1,0:T(8,128)(2,1)}, bf16[256,2048]{1,0:T(8,128)(2,1)S(1)}, u32[]{:S(2)}, u32[]{:S(2)}) %collective-permute-start) | collective-permute-done | bytes 1048608 | tf_op jit(solution)/shard_map/ppermute | solution.py:15
  38.9 42.7 %collective-permute-done.1 = bf16[256,2048]{1,0:T(8,128)(2,1)S(1)} collective-permute-done((bf16[256,2048]{1,0:T(8,128)(2,1)S(1)}, bf16[256,2048]{1,0:T(8,128)(2,1)S(1)}, u32[]{:S(2)}, u32[]{:S(2)}) %collective-permute-start.1) | collective-permute-done | bytes 1048608 | tf_op jit(solution)/shard_map/ppermute | solution.py:15
  81.6 40.6 %collective-permute-done.2 = bf16[256,2048]{1,0:T(8,128)(2,1)S(1)} collective-permute-done((bf16[256,2048]{1,0:T(8,128)(2,1)S(1)}, bf16[256,2048]{1,0:T(8,128)(2,1)S(1)}, u32[]{:S(2)}, u32[]{:S(2)}) %collective-permute-start.2) | collective-permute-done | bytes 1048608 | tf_op jit(solution)/shard_map/ppermute | solution.py:15
  123.2 50.3 %collective-permute-done.3 = bf16[256,2048]{1,0:T(8,128)(2,1)S(1)} collective-permute-done((bf16[256,2048]{1,0:T(8,128)(2,1)S(1)}, bf16[256,2048]{1,0:T(8,128)(2,1)S(1)}, u32[]{:S(2)}, u32[]{:S(2)}) %collective-permute-start.3) | collective-permute-done | bytes 1048608 | tf_op jit(solution)/shard_map/ppermute | solution.py:15
  174.4 50.1 %collective-permute-done.4 = bf16[256,2048]{1,0:T(8,128)(2,1)S(1)} collective-permute-done((bf16[256,2048]{1,0:T(8,128)(2,1)S(1)}, bf16[256,2048]{1,0:T(8,128)(2,1)S(1)}, u32[]{:S(2)}, u32[]{:S(2)}) %collective-permute-start.4) | collective-permute-done | bytes 1048608 | tf_op jit(solution)/shard_map/ppermute | solution.py:15
  225.5 32.9 %collective-permute-done.5 = bf16[256,2048]{1,0:T(8,128)(2,1)} collective-permute-done((bf16[256,2048]{1,0:T(8,128)(2,1)S(1)}, bf16[256,2048]{1,0:T(8,128)(2,1)}, u32[]{:S(2)}, u32[]{:S(2)}) %collective-permute-start.5) | collective-permute-done | bytes 1048608 | tf_op jit(solution)/shard_map/ppermute | solution.py:15
  258.3 27.7 %collective-permute-done.6 = bf16[256,2048]{1,0:T(8,128)(2,1)} collective-permute-done((bf16[256,2048]{1,0:T(8,128)(2,1)}, bf16[256,2048]{1,0:T(8,128)(2,1)}, u32[]{:S(2)}, u32[]{:S(2)}) %collective-permute-start.6) | collective-permute-done | bytes 1048608 | tf_op jit(solution)/shard_map/ppermute | solution.py:15
  286.1 2.3 constant_dynamic-update-slice_fusion.15
  290.7 2.3 constant_dynamic-update-slice_fusion.13
  293.0 2.3 constant_dynamic-update-slice_fusion.12
  295.3 2.3 constant_dynamic-update-slice_fusion.11
  300.9 2.3 constant_dynamic-update-slice_fusion.7
  303.2 2.3 constant_dynamic-update-slice_fusion.6
  311.8 6.1 fusion.4
  318.0 9.3 fusion.11
  327.6 6.2 fusion.10
  334.7 8.1 convolution_bitcast_fusion
  342.9 264.7 %reduce-scatter.8.cloned.1.call-done = f32[2048,256]{1,0:T(8,128)} async-done(((f32[2048,2048]{1,0:T(8,128)}), f32[2048,256]{1,0:T(8,128)}) %reduce-scatter.8.cloned.1.call-update) | async-done | bytes 2097168 | tf_op jit(solution)/shard_map/reduce_scatter | solution.py:57
  607.6 283.0 %reduce-scatter.6.cloned.1.call-done = f32[256,2048]{0,1:T(8,128)} async-done(((f32[2048,2048]{0,1:T(8,128)}), f32[256,2048]{0,1:T(8,128)}) %reduce-scatter.6.cloned.1.call-update) | async-done | bytes 2097168 | tf_op jit(solution)/shard_map/reduce_scatter | solution.py:49
  890.7 6.8 fusion.7
  897.5 102.5 %all-reduce.3.cloned.1.call-done = (f32[256,2048]{0,1:T(8,128)}, f32[2048,256]{1,0:T(8,128)}) async-done(((f32[256,2048]{0,1:T(8,128)}, f32[2048,256]{1,0:T(8,128)}), (f32[256,2048]{0,1:T(8,128)}, f32[2048,256]{1,0:T(8,128)})) %all-reduce.3.cloned.1.call-update) | async-done | bytes 4194320 | tf_op jit(solution)/shard_map/psum | solution.py:58
  1003.5 3.0 broadcast_multiply_fusion
  1006.6 4.7 reduce-scatter.4.cloned.1.call-done
  (55 shorter events, 21.9 us)
Async XLA Ops:
  7.2 292.6 %copy-start = (bf16[256,2048]{1,0:T(8,128)(2,1)S(1)}, bf16[256,2048]{1,0:T(8,128)(2,1)}, u32[]{:S(2)}) copy-start(bf16[256,2048]{1,0:T(8,128)(2,1)} %param.6) | copy-start | bytes 3145732
  7.2 304.7 %all-gather.4.cloned.1.call-start = ((), (), s32[]{:S(2)}) async-start(), calls=%async_computation.3 | async-start | bytes 1572864 | tf_op jit(solution)/shard_map/all_gather | solution.py:10
  7.9 310.1 %all-gather.6.cloned.1.call-start = ((), (), s32[]{:S(2)}) async-start(), calls=%async_computation.4 | async-start | bytes 1572864 | tf_op jit(solution)/shard_map/all_gather | solution.py:11
  8.7 318.9 %all-gather.8.cloned.1.call-start = ((), (), s32[]{:S(2)}) async-start(), calls=%async_computation.5 | async-start | bytes 9437184 | tf_op jit(solution)/shard_map/all_gather | solution.py:25
  9.4 598.2 %reduce-scatter.8.cloned.1.call-start = ((), (), s32[]{:S(2)}) async-start(), calls=%async_computation.8 | async-start | bytes 18874368 | tf_op jit(solution)/shard_map/reduce_scatter | solution.py:57
  9.4 29.5 %collective-permute-start = (bf16[256,2048]{1,0:T(8,128)(2,1)}, bf16[256,2048]{1,0:T(8,128)(2,1)S(1)}, u32[]{:S(2)}, u32[]{:S(2)}) collective-permute-start(bf16[256,2048]{1,0:T(8,128)(2,1)} %param.6), channel_id=1, source_target_pairs={{0,2},{2,4},{4,6},{6,8},{8,10},{10,12},{12,14},{14,0},{1,3},{3,5},... | collective-permute-start | bytes 3145736 | tf_op jit(solution)/shard_map/ppermute | solution.py:15
  38.9 42.7 %collective-permute-start.1 = (bf16[256,2048]{1,0:T(8,128)(2,1)S(1)}, bf16[256,2048]{1,0:T(8,128)(2,1)S(1)}, u32[]{:S(2)}, u32[]{:S(2)}) collective-permute-start(bf16[256,2048]{1,0:T(8,128)(2,1)S(1)} %collective-permute-done), channel_id=1, source_target_pairs={{0,2},{2,4},{4,6},{6,8},{8,10},{10,12},{12,14},{14,0},{1,3},{3,5},... | collective-permute-start | bytes 3145736 | tf_op jit(solution)/shard_map/ppermute | solution.py:15
  81.6 40.6 %collective-permute-start.2 = (bf16[256,2048]{1,0:T(8,128)(2,1)S(1)}, bf16[256,2048]{1,0:T(8,128)(2,1)S(1)}, u32[]{:S(2)}, u32[]{:S(2)}) collective-permute-start(bf16[256,2048]{1,0:T(8,128)(2,1)S(1)} %collective-permute-done.1), channel_id=1, source_target_pairs={{0,2},{2,4},{4,6},{6,8},{8,10},{10,12},{12,14},{14,0},{1,3},{3,5},... | collective-permute-start | bytes 3145736 | tf_op jit(solution)/shard_map/ppermute | solution.py:15
  122.2 1.0 copy-start.1
  123.1 50.3 %collective-permute-start.3 = (bf16[256,2048]{1,0:T(8,128)(2,1)S(1)}, bf16[256,2048]{1,0:T(8,128)(2,1)S(1)}, u32[]{:S(2)}, u32[]{:S(2)}) collective-permute-start(bf16[256,2048]{1,0:T(8,128)(2,1)S(1)} %collective-permute-done.2), channel_id=1, source_target_pairs={{0,2},{2,4},{4,6},{6,8},{8,10},{10,12},{12,14},{14,0},{1,3},{3,5},... | collective-permute-start | bytes 3145736 | tf_op jit(solution)/shard_map/ppermute | solution.py:15
  173.5 1.0 copy-start.3
  174.4 50.1 %collective-permute-start.4 = (bf16[256,2048]{1,0:T(8,128)(2,1)S(1)}, bf16[256,2048]{1,0:T(8,128)(2,1)S(1)}, u32[]{:S(2)}, u32[]{:S(2)}) collective-permute-start(bf16[256,2048]{1,0:T(8,128)(2,1)S(1)} %collective-permute-done.3), channel_id=1, source_target_pairs={{0,2},{2,4},{4,6},{6,8},{8,10},{10,12},{12,14},{14,0},{1,3},{3,5},... | collective-permute-start | bytes 3145736 | tf_op jit(solution)/shard_map/ppermute | solution.py:15
  224.5 1.0 copy-start.5
  225.5 32.9 %collective-permute-start.5 = (bf16[256,2048]{1,0:T(8,128)(2,1)S(1)}, bf16[256,2048]{1,0:T(8,128)(2,1)}, u32[]{:S(2)}, u32[]{:S(2)}) collective-permute-start(bf16[256,2048]{1,0:T(8,128)(2,1)S(1)} %collective-permute-done.4), channel_id=1, source_target_pairs={{0,2},{2,4},{4,6},{6,8},{8,10},{10,12},{12,14},{14,0},{1,3},{3,5},... | collective-permute-start | bytes 3145736 | tf_op jit(solution)/shard_map/ppermute | solution.py:15
  258.3 27.7 %collective-permute-start.6 = (bf16[256,2048]{1,0:T(8,128)(2,1)}, bf16[256,2048]{1,0:T(8,128)(2,1)}, u32[]{:S(2)}, u32[]{:S(2)}) collective-permute-start(bf16[256,2048]{1,0:T(8,128)(2,1)} %collective-permute-done.5), channel_id=1, source_target_pairs={{0,2},{2,4},{4,6},{6,8},{8,10},{10,12},{12,14},{14,0},{1,3},{3,5},... | collective-permute-start | bytes 3145736 | tf_op jit(solution)/shard_map/ppermute | solution.py:15
  258.3 47.2 %copy-start.6 = (bf16[256,2048]{1,0:T(8,128)(2,1)S(1)}, bf16[256,2048]{1,0:T(8,128)(2,1)}, u32[]{:S(2)}) copy-start(bf16[256,2048]{1,0:T(8,128)(2,1)} %copy-done.5) | copy-start | bytes 3145732
  258.3 48.2 %copy-start.4 = (bf16[256,2048]{1,0:T(8,128)(2,1)S(1)}, bf16[256,2048]{1,0:T(8,128)(2,1)}, u32[]{:S(2)}) copy-start(bf16[256,2048]{1,0:T(8,128)(2,1)} %copy-done.3) | copy-start | bytes 3145732
  258.3 49.3 %copy-start.2 = (bf16[256,2048]{1,0:T(8,128)(2,1)S(1)}, bf16[256,2048]{1,0:T(8,128)(2,1)}, u32[]{:S(2)}) copy-start(bf16[256,2048]{1,0:T(8,128)(2,1)} %copy-done.1) | copy-start | bytes 3145732
  327.3 7.4 copy-start.7
  327.3 563.3 %reduce-scatter.6.cloned.1.call-start = ((), (), s32[]{:S(2)}) async-start(), calls=%async_computation.7 | async-start | bytes 18874368 | tf_op jit(solution)/shard_map/reduce_scatter | solution.py:49
  333.8 1.0 copy-start.8
  342.8 547.9 %copy-start.9 = (bf16[256,2048]{0,1:T(8,128)(2,1)S(1)}, bf16[256,2048]{0,1:T(8,128)(2,1)}, u32[]{:S(2)}) copy-start(bf16[256,2048]{0,1:T(8,128)(2,1)} %copy-done.8) | copy-start | bytes 3145732
  342.8 657.2 %all-reduce.3.cloned.1.call-start = ((), (), s32[]{:S(2)}) async-start(), calls=%async_computation.9 | async-start | bytes 8388608 | tf_op jit(solution)/shard_map/psum | solution.py:58
  890.6 120.6 %reduce-scatter.4.cloned.1.call-start = ((), (), s32[]{:S(2)}) async-start(), calls=%async_computation.6 | async-start | bytes 1572864 | tf_op jit(solution)/shard_map/reduce_scatter | solution.py:33
Sparse Core Ops, SparseCore 0:
  9.5 11.7 all-gather.3
  22.9 10.1 all-gather.5
  35.1 194.4 all-gather.7
  327.5 280.1 reduce-scatter.7
  611.2 279.3 reduce-scatter.5
  892.9 107.0 all-reduce.2
  1002.8 8.3 reduce-scatter.3
